TPU v7x, 32 devices: a whole 2x2x4 slice. The times are simulated.
32 devices in a mesh: ep: 8 (over z, core), tp: 4 (over y, x).
Axes of the slice: x: 2, y: 2, z: 4, core: 2. Of those that a mesh axis runs over, the one named last changes fastest.
Arguments:
- tokens: bfloat16 [512, 2048], P('ep', 'tp'), as said below
- mix_gain: float32 [2048], replicated, may hold values from 0.1 to 1.9
- w_in: bfloat16 [2048, 1024], P(None, 'tp'), may hold values from -0.125 to 0.125
- a_real: float32 [64, 64], P('tp'), may hold values from -1 to -0.1
- a_imag: float32 [64, 64], P('tp'), may hold values from -3.140625 to 3.140625
- log_step: float32 [64], P('tp'), may hold values from -3 to 0
- b_coef: float32 [2, 64, 64, 16], P(None, 'tp'), may hold values from -2.5 to 2.5
- output_coefficients: float32 [2, 64, 16, 64], P(None, 'tp'), may hold values from -1.25 to 1.25
- skip: float32 [1024], P('tp'), may hold values from -6 to 6
- w_out: bfloat16 [1024, 2048], P('tp'), may hold values from -0.1875 to 0.1875
- state: float32 [2, 512, 64, 64], P(None, 'ep', 'tp'), may hold values from -6 to 6
- ffn_gain: float32 [2048], replicated, may hold values from 0.1 to 1.9
- w_gate: bfloat16 [16, 2048, 4096], P('ep', None, 'tp'), may hold values from -0.125 to 0.125
- w_up: bfloat16 [16, 2048, 4096], P('ep', None, 'tp'), may hold values from -0.125 to 0.125
- w_down: bfloat16 [16, 4096, 2048], P('ep', 'tp'), may hold values from -0.09375 to 0.09375
- expert_ids: int32 [512, 2], P('ep'), may hold values from 0 to 15, all different within a row; in each aligned block of 64 rows (0 to 63, 64 to 127, ...) at most 16 rows name the same one
- route_weights: float32 [512, 2], P('ep'), may hold values from 0.3 to 1
Outputs:
- out: bfloat16 [512, 2048], P('ep', 'tp')
- new_state: float32 [2, 512, 64, 64], P(None, 'ep', 'tp')
Inputs may be any that keep to these rules, and one draw needn't show every extreme that they name: `expert_ids`: A token's 2 experts differ. Among the 64 rows of one index of ep no expert is named more than 16 times, a bound that some block reaches. `tokens`: feature scales differ along the model width.
All inputs are finite; a program needn't handle non-finite values.
Results may differ from a plain program's by a relative error of at most 0.007.
Values may be sent and summed in bfloat16 or wider, within the bound.
A program may use at most 64 MiB of HBM per device.

v0:
```python
import jax
import jax.numpy as jnp
from jax import lax
from jax.sharding import PartitionSpec as P

epsilon = 1e-06
highest_precision = lax.Precision.HIGHEST


def rms_norm(values, gain):
    scaled = values * lax.rsqrt(jnp.mean(values * values, axis=-1, keepdims=True) + epsilon)
    return scaled * gain


def state_update(drive, a_real, a_imag, log_step, b_coef, output_coefficients, skip, state):
    count = drive.shape[0]
    groups = a_real.shape[0]
    drive_float = drive.astype(jnp.float32)
    grouped = drive_float.reshape(count, groups, -1)
    step_size = jnp.exp(log_step)[:, None]
    magnitude = jnp.exp(step_size * a_real)
    decay_re = magnitude * jnp.cos(step_size * a_imag)
    decay_imaginary = magnitude * jnp.sin(step_size * a_imag)
    denominator = a_real * a_real + a_imag * a_imag
    shifted = decay_re - 1.0
    factor_re = (shifted * a_real + decay_imaginary * a_imag) / denominator
    factor_im = (decay_imaginary * a_real - shifted * a_imag) / denominator
    coef_re = factor_re[..., None] * b_coef[0] - factor_im[..., None] * b_coef[1]
    coefficient_imaginary = factor_re[..., None] * b_coef[1] + factor_im[..., None] * b_coef[0]
    push_re = jnp.einsum("gpc,sgc->sgp", coef_re, grouped, precision=highest_precision)
    push_im = jnp.einsum(
        "gpc,sgc->sgp", coefficient_imaginary, grouped, precision=highest_precision
    )
    state_real = decay_re * state[0] - decay_imaginary * state[1] + push_re
    state_imaginary = decay_re * state[1] + decay_imaginary * state[0] + push_im
    state_readout = jnp.einsum(
        "amz,daz->dam", output_coefficients[0], state_real, precision=highest_precision
    ) - jnp.einsum(
        "amz,daz->dam", output_coefficients[1], state_imaginary, precision=highest_precision
    )
    mixed = state_readout.reshape(count, -1) + skip * drive_float
    return (jax.nn.gelu(mixed).astype(jnp.bfloat16), jnp.stack([state_real, state_imaginary]))


def slot_table(expert_ids, experts, capacity):
    flat_ids = expert_ids.reshape(-1)
    onehot = (flat_ids[:, None] == jnp.arange(experts, dtype=jnp.int32)[None, :]).astype(jnp.int32)
    ranks = jnp.cumsum(onehot, axis=0) - 1
    slot_rank = jnp.sum(onehot * ranks, axis=1)
    slots = flat_ids * capacity + slot_rank
    return (slots[:, None] == jnp.arange(experts * capacity, dtype=jnp.int32)[None, :]).astype(
        jnp.float32
    )


def local(
    tokens,
    mix_gain,
    w_in,
    a_real,
    a_imag,
    log_step,
    b_coef,
    output_coefficients,
    skip,
    w_out,
    state,
    ffn_gain,
    w_gate,
    w_up,
    w_down,
    expert_ids,
    route_weights,
):
    seq_count = tokens.shape[0]
    width = tokens.shape[1]
    top_count = expert_ids.shape[1]
    ep_count = lax.axis_size("ep")
    tp_count = lax.axis_size("tp")
    model_width = width * tp_count
    local_experts = w_gate.shape[0]
    experts = local_experts * ep_count
    capacity = max(2, 2 * seq_count * top_count // experts)
    col_start = lax.axis_index("tp") * width
    whole_rows = lax.all_gather(tokens, "tp", axis=1, tiled=True)
    tok_float = whole_rows.astype(jnp.float32)
    normed = rms_norm(tok_float, mix_gain).astype(jnp.bfloat16)
    drive = jnp.dot(normed, w_in, preferred_element_type=jnp.float32).astype(jnp.bfloat16)
    mixed, new_state = state_update(
        drive, a_real, a_imag, log_step, b_coef, output_coefficients, skip, state
    )
    partial_mix = jnp.dot(mixed, w_out, preferred_element_type=jnp.float32)
    placed = slot_table(expert_ids, experts, capacity)
    per_token = (
        placed.reshape(seq_count, top_count, experts * capacity).sum(axis=1).astype(jnp.bfloat16)
    )
    mix_full = lax.psum(partial_mix, "tp")
    resid_full = (tok_float + mix_full).astype(jnp.bfloat16)
    normed2 = rms_norm(resid_full.astype(jnp.float32), ffn_gain).astype(jnp.bfloat16)
    resid_own = lax.dynamic_slice_in_dim(resid_full, col_start, width, 1)
    send_buffer = jnp.dot(per_token.T, normed2, preferred_element_type=jnp.float32).astype(
        jnp.bfloat16
    )
    send_buffer = send_buffer.reshape(ep_count, local_experts, capacity, model_width)
    slot_rows = lax.all_to_all(send_buffer, "ep", split_axis=0, concat_axis=0, tiled=True)
    gate_vals = jnp.einsum("njcd,jdf->njcf", slot_rows, w_gate, preferred_element_type=jnp.float32)
    up_vals = jnp.einsum("njcd,jdf->njcf", slot_rows, w_up, preferred_element_type=jnp.float32)
    hidden = (jax.nn.silu(gate_vals) * up_vals).astype(jnp.bfloat16)
    partial_out = jnp.einsum("njcf,jfd->njcd", hidden, w_down, preferred_element_type=jnp.float32)
    expert_result = lax.psum_scatter(
        partial_out.astype(jnp.bfloat16), "tp", scatter_dimension=3, tiled=True
    )
    returned_rows = lax.all_to_all(expert_result, "ep", split_axis=0, concat_axis=0, tiled=True)
    returned_rows = returned_rows.reshape(experts * capacity, width).astype(jnp.float32)
    weighted = placed * route_weights.reshape(-1)[:, None]
    combined = jnp.dot(weighted, returned_rows, precision=highest_precision)
    combined = combined.reshape(seq_count, top_count, width).sum(axis=1)
    out = (resid_own.astype(jnp.float32) + combined).astype(jnp.bfloat16)
    return (out, new_state)


def solution(mesh):
    in_specs = (
        P("ep", "tp"),
        P(),
        P(None, "tp"),
        P("tp", None),
        P("tp", None),
        P("tp"),
        P(None, "tp", None, None),
        P(None, "tp", None, None),
        P("tp"),
        P("tp", None),
        P(None, "ep", "tp", None),
        P(),
        P("ep", None, "tp"),
        P("ep", None, "tp"),
        P("ep", "tp", None),
        P("ep", None),
        P("ep", None),
    )
    out_specs = (P("ep", "tp"), P(None, "ep", "tp", None))
    return jax.shard_map(local, mesh=mesh, in_specs=in_specs, out_specs=out_specs, check_vma=False)
```

profile of v0, /device:TPU:0, one launch (start us, length us, event | category | flops | bytes accessed | tf_op | source)
XLA Modules:
  0.0 168.2 jit_solution(7657873128458054456)
XLA Ops:
  7.2 0.0 copy-start
  7.2 0.0 copy-start.1
  7.2 0.0 copy-start.5
  7.2 0.0 copy-start.3
  7.2 0.0 copy-start.2
  7.2 0.0 all-reduce.2.cloned.1.call-start
  7.3 10.9 %all_gather.3 = bf16[64,2048]{1,0:T(8,128)(2,1)S(1)} all-gather(bf16[64,512]{1,0:T(8,128)(2,1)} %param.17), channel_id=1, replica_groups=mesh['ep'=8,'tp'=4] {'tp'}, dimensions={1}, use_global_device_ids=true | all-gather | bytes 327680 | tf_op jit(solution)/shard_map/all_gather | solution.py:85
  18.2 0.2 fusion.31
  18.3 1.6 convolution_convert_fusion.1
  19.9 0.1 copy.68
  20.0 0.7 exp.10
  20.7 1.3 fusion.87
  22.0 0.8 fusion.80
  22.8 1.6 fusion.24
  24.4 1.6 fusion.25
  26.1 1.8 %fusion.43 = f32[16,64,16]{1,2,0:T(8,128)S(1)} fusion(f32[64,16,64]{2,0,1:T(8,128)S(1)} %fusion.25, f32[2,16,16,64]{3,2,1,0:T(8,128)} %param.24), kind=kOutput, calls=%fused_computation.43 | convolution fusion | flops 12582912 | bytes 458752 | tf_op jit(solution)/shard_map/amz,daz->dam/dot_general | solution.py:36
  27.9 0.9 convolution_subtract_fusion
  28.9 0.1 copy.69
  29.0 1.1 fusion.72
  30.1 0.0 all-reduce.2.cloned.1.call-update
  30.1 0.0 reduce-scatter.2.cloned.1.call-start
  30.1 0.1 copy.70
  30.2 0.1 eq.49
  30.4 0.1 fusion.67
  30.5 0.2 reduce_window_sum.11
  30.6 0.2 select_reduce_fusion
  30.8 0.1 reduce_sum.49
  31.0 0.1 copy.71
  31.0 0.1 convert_reduce_fusion
  31.2 44.7 %all-reduce.2.cloned.1.call-done = f32[64,2048]{1,0:T(8,128)} async-done(((f32[64,2048]{1,0:T(8,128)}), f32[64,2048]{1,0:T(8,128)}) %all-reduce.2.cloned.1.call-update) | async-done | bytes 524304 | tf_op jit(solution)/shard_map/psum | solution.py:97
  75.9 1.2 fusion.28
  77.1 0.5 convolution_convert_fusion
  77.6 0.0 slice-start.2
  77.6 31.2 %all_to_all.10 = bf16[8,2,16,2048]{3,2,1,0:T(8,128)(2,1)S(1)} all-to-all(bf16[8,2,16,2048]{3,2,1,0:T(8,128)(2,1)S(1)} %bitcast.107), channel_id=1, replica_groups=mesh['ep'=8,'tp'=4] {'ep'}, dimensions={0} | all-to-all | bytes 2097152 | tf_op jit(solution)/shard_map/all_to_all | solution.py:105
  108.9 4.8 %fusion.12 = f32[8,2,16,1024]{3,2,0,1:T(8,128)S(1)} fusion(bf16[2,2048,1024]{2,1,0:T(8,128)(2,1)} %param.29, bf16[8,2,16,2048]{3,2,1,0:T(8,128)(2,1)S(1)} %all_to_all.10), kind=kOutput, calls=%fused_computation.9 | convolution fusion | flops 1073741824 | bytes 10485760 | tf_op jit(solution)/shard_map/njcd,jdf->njcf/dot_general | solution.py:106
  113.7 0.0 slice-start.1
  113.7 1.4 fusion.21
  115.1 1.0 slice-done.1
  116.1 2.2 %fusion.9 = bf16[8,2,16,2048]{3,2,0,1:T(8,128)(2,1)} fusion(bf16[8,2,16,1024]{3,2,0,1:T(8,128)(2,1)S(1)} %fusion.21, bf16[2,1024,2048]{2,1,0:T(8,128)(2,1)S(1)} %bitcast.104), kind=kOutput, calls=%fused_computation.8 | convolution fusion | flops 1074266112 | bytes 9961472 | tf_op jit(solution)/shard_map/njcf,jfd->njcd/dot_general | solution.py:109
  118.4 0.0 reduce-scatter.2.cloned.1.call-update
  118.4 26.0 %reduce-scatter.2.cloned.1.call-done = bf16[8,2,16,512]{3,2,0,1:T(8,128)(2,1)} async-done(((bf16[8,2,16,2048]{3,2,0,1:T(8,128)(2,1)}), bf16[8,2,16,512]{3,2,0,1:T(8,128)(2,1)}) %reduce-scatter.2.cloned.1.call-update) | async-done | bytes 262160 | tf_op jit(solution)/shard_map/reduce_scatter | solution.py:110
  144.4 1.7 copy.74
  146.1 4.6 %all-to-all-start.1 = ((bf16[8,2,16,512]{3,2,1,0:T(8,128)(2,1)}), bf16[8,2,16,512]{3,2,1,0:T(8,128)(2,1)S(1)}, u32[]{:S(2)}, u32[]{:S(2)}) async-start(bf16[8,2,16,512]{3,2,1,0:T(8,128)(2,1)} %copy.74), calls=%async_computation.2 | async-start | bytes 524288 | tf_op jit(solution)/shard_map/all_to_all | solution.py:113
  150.7 0.1 pad_maximum_fusion
  150.8 1.6 copy.75
  152.4 8.0 %all-to-all-done.1 = bf16[8,2,16,512]{3,2,1,0:T(8,128)(2,1)S(1)} async-done(((bf16[8,2,16,512]{3,2,1,0:T(8,128)(2,1)}), bf16[8,2,16,512]{3,2,1,0:T(8,128)(2,1)S(1)}, u32[]{:S(2)}, u32[]{:S(2)}) %all-to-all-start.1) | async-done | bytes 262176 | tf_op jit(solution)/shard_map/all_to_all | solution.py:113
  160.4 0.3 convolution_reduce_fusion
  160.8 0.7 add_convert_fusion
  (17 shorter events, 0.0 us)
Async XLA Ops:
  7.2 21.8 %copy-start = (bf16[256,2048]{1,0:T(8,128)(2,1)S(1)}, bf16[256,2048]{1,0:T(8,128)(2,1)}, u32[]{:S(2)}) copy-start(bf16[256,2048]{1,0:T(8,128)(2,1)} %param.26) | copy-start | bytes 3145732
  7.2 20.7 %copy-start.1 = (f32[2,16,16,64]{3,2,1,0:T(8,128)S(1)}, f32[2,16,16,64]{3,2,1,0:T(8,128)}, u32[]{:S(2)}) copy-start(f32[2,16,16,64]{3,2,1,0:T(8,128)} %param.24) | copy-start | bytes 393220
  7.2 21.8 %copy-start.5 = (f32[256]{0:T(256)S(1)}, f32[256]{0:T(256)}, u32[]{:S(2)}) copy-start(f32[256]{0:T(256)} %param.25) | copy-start | bytes 3076
  7.2 22.9 %copy-start.3 = (s32[64,2]{0,1:T(2,128)S(1)}, s32[64,2]{0,1:T(2,128)}, u32[]{:S(2)}) copy-start(s32[64,2]{0,1:T(2,128)} %param.32) | copy-start | bytes 1540
  7.2 69.9 %copy-start.2 = (f32[2048]{0:T(1024)S(1)}, f32[2048]{0:T(1024)}, u32[]{:S(2)}) copy-start(f32[2048]{0:T(1024)} %param.28) | copy-start | bytes 24580
  7.2 68.7 %all-reduce.2.cloned.1.call-start = ((), (), s32[]{:S(2)}) async-start(), calls=%async_computation.3 | async-start | bytes 1048576 | tf_op jit(solution)/shard_map/psum | solution.py:97
  30.1 114.4 %reduce-scatter.2.cloned.1.call-start = ((), (), s32[]{:S(2)}) async-start(), calls=%async_computation.4 | async-start | bytes 1310720 | tf_op jit(solution)/shard_map/reduce_scatter | solution.py:110
  77.6 36.0 %slice-start.2 = ((s8[8388608]{0:T(1024)(128)(4,1)}), s8[4194304]{0:T(1024)(128)(4,1)S(1)}, s32[]{:S(2)}) async-start(s8[8388608]{0:T(1024)(128)(4,1)} %bitcast.112), calls=%async_computation.7 | async-start | bytes 8388608
  108.9 4.8 %slice-start.3 = ((s8[8388608]{0:T(1024)(128)(4,1)}), s8[4194304]{0:T(1024)(128)(4,1)S(1)}, s32[]{:S(2)}) async-start(s8[8388608]{0:T(1024)(128)(4,1)} %bitcast.112), calls=%async_computation.8 | async-start | bytes 8388608
  108.9 6.3 %slice-start = ((s8[8388608]{0:T(1024)(128)(4,1)}), s8[4194304]{0:T(1024)(128)(4,1)S(1)}, s32[]{:S(2)}) async-start(s8[8388608]{0:T(1024)(128)(4,1)} %bitcast.103), calls=%async_computation.5 | async-start | bytes 8388608
  113.7 2.5 %slice-start.1 = ((s8[8388608]{0:T(1024)(128)(4,1)}), s8[4194304]{0:T(1024)(128)(4,1)S(1)}, s32[]{:S(2)}) async-start(s8[8388608]{0:T(1024)(128)(4,1)} %bitcast.103), calls=%async_computation.6 | async-start | bytes 8388608
  116.1 44.3 %copy-start.4 = (f32[64,2]{0,1:T(2,128)S(1)}, f32[64,2]{0,1:T(2,128)}, u32[]{:S(2)}) copy-start(f32[64,2]{0,1:T(2,128)} %param.33) | copy-start | bytes 1540
  146.1 14.3 %all-to-all-start.1 = ((bf16[8,2,16,512]{3,2,1,0:T(8,128)(2,1)}), bf16[8,2,16,512]{3,2,1,0:T(8,128)(2,1)S(1)}, u32[]{:S(2)}, u32[]{:S(2)}) async-start(bf16[8,2,16,512]{3,2,1,0:T(8,128)(2,1)} %copy.74), calls=%async_computation.2 | async-start | bytes 524288 | tf_op jit(solution)/shard_map/all_to_all | solution.py:113
Sparse Core Ops, SparseCore 0:
  30.2 45.6 all-reduce.1
  118.5 25.8 reduce-scatter.1
where the time goes:
time: 169 us; the launch traced here: 168 us
  waiting for transfers between devices  78.8 us (47%)
  blocking collectives  42.1 us (25%)
  matrix products  18 us (11%)
  between operations  14.3 us (8%)
  local copies, waits for them, and re-layouts  6.87 us (4%)
  starting transfers between devices  4.69 us (3%)
  other arithmetic  3.53 us (2%)
    psum x1, waiting for transfers between devices, local(): mix_full = lax.psum(partial_mix, 'tp')  44.7 us
    all_to_all x1, blocking collectives, local(): lax.all_to_all(send_buffer, 'ep', split_axis=0, concat_axis=0, tiled=True)  31.2 us
    reduce_scatter x1, waiting for transfers between devices, local(): lax.psum_scatter(partial_out.astype(jnp.bfloat16), 'tp', scatter_dimensio...  26 us
    all_gather x1, blocking collectives, local(): whole_rows = lax.all_gather(tokens, 'tp', axis=1, tiled=True)  10.9 us
    all_to_all x1, waiting for transfers between devices, local(): lax.all_to_all(expert_result, 'ep', split_axis=0, concat_axis=0, tiled=True)  8.01 us
    dot_general x1, matrix products, local(): jnp.einsum('njcd,jdf->njcf', slot_rows, w_gate, preferred_element_type=jn...  4.78 us
    all_to_all x1, starting transfers between devices, local(): lax.all_to_all(expert_result, 'ep', split_axis=0, concat_axis=0, tiled=True)  4.61 us
  transfers between devices with their start and end apart: 3, of which 3 were waited for; matrix products, arithmetic and copies ran while one was open for 2% of the time, Pallas kernels for 0%

commit v1 on v0

--- a/solution.py
+++ b/solution.py
@@ -94,7 +94,7 @@
     per_token = (
         placed.reshape(seq_count, top_count, experts * capacity).sum(axis=1).astype(jnp.bfloat16)
     )
-    mix_full = lax.psum(partial_mix, "tp")
+    mix_full = jnp.sum(lax.all_gather(partial_mix, "tp"), axis=0)
     resid_full = (tok_float + mix_full).astype(jnp.bfloat16)
     normed2 = rms_norm(resid_full.astype(jnp.float32), ffn_gain).astype(jnp.bfloat16)
     resid_own = lax.dynamic_slice_in_dim(resid_full, col_start, width, 1)

time: 169 us -> 159 us (0.941)
  waiting for transfers between devices: 78.8 us -> 68.6 us
    psum x1 -> x0, waiting for transfers between devices: 44.7 us -> none  [local(): mix_full = lax.psum(partial_mix, 'tp')]
    all_gather x0 -> x1, waiting for transfers between devices: none -> 34.5 us  [local(): mix_full = jnp.sum(lax.all_gather(partial_mix, 'tp'), axis=0)]
    reduce_sum x0 -> x1, other arithmetic: none -> 1.76 us  [local(): mix_full = jnp.sum(lax.all_gather(partial_mix, 'tp'), axis=0)]
where the time goes in v1:
time: 159 us
  waiting for transfers between devices  68.6 us (43%)
  blocking collectives  42.1 us (26%)
  matrix products  17.9 us (11%)
  between operations  14.3 us (9%)
  local copies, waits for them, and re-layouts  6.88 us (4%)
  starting transfers between devices  4.69 us (3%)
  other arithmetic  4.25 us (3%)
    all_gather x1, waiting for transfers between devices, local(): mix_full = jnp.sum(lax.all_gather(partial_mix, 'tp'), axis=0)  34.5 us
    all_to_all x1, blocking collectives, local(): lax.all_to_all(send_buffer, 'ep', split_axis=0, concat_axis=0, tiled=True)  31.2 us
    reduce_scatter x1, waiting for transfers between devices, local(): lax.psum_scatter(partial_out.astype(jnp.bfloat16), 'tp', scatter_dimensio...  26 us
    all_gather x1, blocking collectives, local(): whole_rows = lax.all_gather(tokens, 'tp', axis=1, tiled=True)  10.9 us
    all_to_all x1, waiting for transfers between devices, local(): lax.all_to_all(expert_result, 'ep', split_axis=0, concat_axis=0, tiled=True)  8.01 us
    dot_general x1, matrix products, local(): jnp.einsum('njcd,jdf->njcf', slot_rows, w_gate, preferred_element_type=jn...  4.78 us
    all_to_all x1, starting transfers between devices, local(): lax.all_to_all(expert_result, 'ep', split_axis=0, concat_axis=0, tiled=True)  4.61 us
  transfers between devices with their start and end apart: 3, of which 3 were waited for; matrix products, arithmetic and copies ran while one was open for 2% of the time, Pallas kernels for 0%

profile of v1, /device:TPU:0, one launch (start us, length us, event | category | flops | bytes accessed | tf_op | source)
XLA Modules:
  0.0 158.8 jit_solution(669779991791791203)
XLA Ops:
  7.2 0.0 copy-start
  7.2 0.0 copy-start.1
  7.2 0.0 copy-start.5
  7.2 0.0 copy-start.3
  7.2 0.0 all-gather.3.cloned.1.call-start
  7.3 10.9 %all_gather.9 = bf16[64,2048]{1,0:T(8,128)(2,1)S(1)} all-gather(bf16[64,512]{1,0:T(8,128)(2,1)} %param.17), channel_id=1, replica_groups=mesh['ep'=8,'tp'=4] {'tp'}, dimensions={1}, use_global_device_ids=true | all-gather | bytes 327680 | tf_op jit(solution)/shard_map/all_gather | solution.py:85
  18.2 0.2 fusion.31
  18.3 1.6 convolution_convert_fusion.1
  19.9 0.1 copy.68
  20.0 0.7 exp.10
  20.7 1.3 fusion.87
  22.0 0.8 fusion.80
  22.8 1.6 %fusion.24 = f32[64,16,64]{2,0,1:T(8,128)S(1)} fusion(bf16[64,16,16]{0,2,1:T(8,128)(2,1)S(1)} %bitcast.111, f32[1,64,16,64]{3,2,1,0:T(8,128)S(1)} %get-tuple-element.15, f32[1,64,16,64]{3,2,1,0:T(8,128)S(1)} %get-tuple-element.14, f32[16,64]{1,0:T(8,128)S(1)} %get-tuple-element.17, f32[16,64]{1,0:T(8,128)S(1)} %get-tuple-element.18, ...), kind=kOutput, calls=%fused_computation.14 | convolution fusion | flops 12894208 | bytes 966656 | tf_op jit(solution)/shard_map/gpc,sgc->sgp/dot_general | solution.py:31
  24.4 1.6 %fusion.25 = f32[64,16,64]{2,0,1:T(8,128)S(1)} fusion(bf16[64,16,16]{0,2,1:T(8,128)(2,1)S(1)} %bitcast.112, f32[1,64,16,64]{3,2,1,0:T(8,128)S(1)} %get-tuple-element.15, f32[1,64,16,64]{3,2,1,0:T(8,128)S(1)} %get-tuple-element.14, f32[16,64]{1,0:T(8,128)S(1)} %get-tuple-element.17, f32[16,64]{1,0:T(8,128)S(1)} %get-tuple-element.18, ...), kind=kOutput, calls=%fused_computation.16 | convolution fusion | flops 12894208 | bytes 966656 | tf_op jit(solution)/shard_map/gpc,sgc->sgp/dot_general | solution.py:30
  26.1 1.8 %fusion.43 = f32[16,64,16]{1,2,0:T(8,128)S(1)} fusion(f32[64,16,64]{2,0,1:T(8,128)S(1)} %fusion.25, f32[2,16,16,64]{3,2,1,0:T(8,128)} %param.24), kind=kOutput, calls=%fused_computation.43 | convolution fusion | flops 12582912 | bytes 458752 | tf_op jit(solution)/shard_map/amz,daz->dam/dot_general | solution.py:36
  27.9 0.9 convolution_subtract_fusion
  28.8 0.1 copy.69
  29.0 1.1 fusion.72
  30.1 0.0 all-gather.3.cloned.1.call-update
  30.1 0.0 reduce-scatter.2.cloned.1.call-start
  30.1 0.1 copy.70
  30.2 0.1 eq.49
  30.4 0.1 fusion.67
  30.5 0.2 reduce_window_sum.11
  30.6 0.2 select_reduce_fusion
  30.8 0.1 reduce_sum.59
  31.0 0.1 copy.71
  31.0 0.1 convert_reduce_fusion
  31.2 34.5 %all-gather.3.cloned.1.call-done = f32[256,2048]{1,0:T(8,128)} async-done(((f32[64,2048]{1,0:T(8,128)}), f32[256,2048]{1,0:T(8,128)}) %all-gather.3.cloned.1.call-update) | async-done | bytes 2097168 | tf_op jit(solution)/shard_map/all_gather | solution.py:97
  65.7 1.8 %reduce_sum.57 = f32[64,2048]{1,0:T(8,128)S(1)} reduce(f32[4,64,2048]{2,1,0:T(8,128)} %bitcast.109, f32[]{:T(128)} %constant.14.clone.1), dimensions={0}, to_apply=%region_1.0 | reduce | flops 393216 | bytes 2621444 | tf_op jit(solution)/shard_map/reduce_sum | solution.py:97
  67.4 0.2 fusion.28
  67.6 0.5 convolution_convert_fusion
  68.1 0.0 slice-start.2
  68.1 31.2 %all_to_all.10 = bf16[8,2,16,2048]{3,2,1,0:T(8,128)(2,1)S(1)} all-to-all(bf16[8,2,16,2048]{3,2,1,0:T(8,128)(2,1)S(1)} %bitcast.108), channel_id=1, replica_groups=mesh['ep'=8,'tp'=4] {'ep'}, dimensions={0} | all-to-all | bytes 2097152 | tf_op jit(solution)/shard_map/all_to_all | solution.py:105
  99.4 4.8 %fusion.12 = f32[8,2,16,1024]{3,2,0,1:T(8,128)S(1)} fusion(bf16[2,2048,1024]{2,1,0:T(8,128)(2,1)} %param.29, bf16[8,2,16,2048]{3,2,1,0:T(8,128)(2,1)S(1)} %all_to_all.10), kind=kOutput, calls=%fused_computation.9 | convolution fusion | flops 1073741824 | bytes 10485760 | tf_op jit(solution)/shard_map/njcd,jdf->njcf/dot_general | solution.py:106
  104.2 0.0 slice-start.1
  104.2 1.4 fusion.21
  105.6 1.0 slice-done.1
  106.7 2.2 %fusion.9 = bf16[8,2,16,2048]{3,2,0,1:T(8,128)(2,1)} fusion(bf16[8,2,16,1024]{3,2,0,1:T(8,128)(2,1)S(1)} %fusion.21, bf16[2,1024,2048]{2,1,0:T(8,128)(2,1)S(1)} %bitcast.105), kind=kOutput, calls=%fused_computation.8 | convolution fusion | flops 1074266112 | bytes 9961472 | tf_op jit(solution)/shard_map/njcf,jfd->njcd/dot_general | solution.py:109
  108.9 0.0 reduce-scatter.2.cloned.1.call-update
  108.9 26.0 %reduce-scatter.2.cloned.1.call-done = bf16[8,2,16,512]{3,2,0,1:T(8,128)(2,1)} async-done(((bf16[8,2,16,2048]{3,2,0,1:T(8,128)(2,1)}), bf16[8,2,16,512]{3,2,0,1:T(8,128)(2,1)}) %reduce-scatter.2.cloned.1.call-update) | async-done | bytes 262160 | tf_op jit(solution)/shard_map/reduce_scatter | solution.py:110
  135.0 1.7 %copy.74 = bf16[8,2,16,512]{3,2,1,0:T(8,128)(2,1)} copy(bf16[8,2,16,512]{3,2,0,1:T(8,128)(2,1)} %reduce-scatter.2.cloned.1.call-done) | data formatting | bytes 524288 | tf_op jit(solution)/shard_map/reduce_scatter | solution.py:110
  136.6 4.6 %all-to-all-start.1 = ((bf16[8,2,16,512]{3,2,1,0:T(8,128)(2,1)}), bf16[8,2,16,512]{3,2,1,0:T(8,128)(2,1)S(1)}, u32[]{:S(2)}, u32[]{:S(2)}) async-start(bf16[8,2,16,512]{3,2,1,0:T(8,128)(2,1)} %copy.74), calls=%async_computation.2 | async-start | bytes 524288 | tf_op jit(solution)/shard_map/all_to_all | solution.py:113
  141.2 0.1 pad_maximum_fusion
  141.3 1.6 copy.75
  142.9 8.0 %all-to-all-done.1 = bf16[8,2,16,512]{3,2,1,0:T(8,128)(2,1)S(1)} async-done(((bf16[8,2,16,512]{3,2,1,0:T(8,128)(2,1)}), bf16[8,2,16,512]{3,2,1,0:T(8,128)(2,1)S(1)}, u32[]{:S(2)}, u32[]{:S(2)}) %all-to-all-start.1) | async-done | bytes 262176 | tf_op jit(solution)/shard_map/all_to_all | solution.py:113
  150.9 0.3 convolution_reduce_fusion
  151.3 0.7 add_convert_fusion
  (18 shorter events, 0.1 us)
Async XLA Ops:
  7.2 21.8 %copy-start = (bf16[256,2048]{1,0:T(8,128)(2,1)S(1)}, bf16[256,2048]{1,0:T(8,128)(2,1)}, u32[]{:S(2)}) copy-start(bf16[256,2048]{1,0:T(8,128)(2,1)} %param.26) | copy-start | bytes 3145732
  7.2 20.7 %copy-start.1 = (f32[2,16,16,64]{3,2,1,0:T(8,128)S(1)}, f32[2,16,16,64]{3,2,1,0:T(8,128)}, u32[]{:S(2)}) copy-start(f32[2,16,16,64]{3,2,1,0:T(8,128)} %param.24) | copy-start | bytes 393220
  7.2 21.8 %copy-start.5 = (f32[256]{0:T(256)S(1)}, f32[256]{0:T(256)}, u32[]{:S(2)}) copy-start(f32[256]{0:T(256)} %param.25) | copy-start | bytes 3076
  7.2 22.9 %copy-start.3 = (s32[64,2]{0,1:T(2,128)S(1)}, s32[64,2]{0,1:T(2,128)}, u32[]{:S(2)}) copy-start(s32[64,2]{0,1:T(2,128)} %param.32) | copy-start | bytes 1540
  7.2 60.4 %copy-start.2 = (f32[2048]{0:T(1024)S(1)}, f32[2048]{0:T(1024)}, u32[]{:S(2)}) copy-start(f32[2048]{0:T(1024)} %param.28) | copy-start | bytes 24580
  7.2 58.4 %all-gather.3.cloned.1.call-start = ((), (), s32[]{:S(2)}) async-start(), calls=%async_computation.4 | async-start | bytes 2621440 | tf_op jit(solution)/shard_map/all_gather | solution.py:97
  30.1 104.9 %reduce-scatter.2.cloned.1.call-start = ((), (), s32[]{:S(2)}) async-start(), calls=%async_computation.3 | async-start | bytes 1310720 | tf_op jit(solution)/shard_map/reduce_scatter | solution.py:110
  68.1 36.0 %slice-start.2 = ((s8[8388608]{0:T(1024)(128)(4,1)}), s8[4194304]{0:T(1024)(128)(4,1)S(1)}, s32[]{:S(2)}) async-start(s8[8388608]{0:T(1024)(128)(4,1)} %bitcast.114), calls=%async_computation.7 | async-start | bytes 8388608
  99.4 4.8 %slice-start.3 = ((s8[8388608]{0:T(1024)(128)(4,1)}), s8[4194304]{0:T(1024)(128)(4,1)S(1)}, s32[]{:S(2)}) async-start(s8[8388608]{0:T(1024)(128)(4,1)} %bitcast.114), calls=%async_computation.8 | async-start | bytes 8388608
  99.4 6.3 %slice-start = ((s8[8388608]{0:T(1024)(128)(4,1)}), s8[4194304]{0:T(1024)(128)(4,1)S(1)}, s32[]{:S(2)}) async-start(s8[8388608]{0:T(1024)(128)(4,1)} %bitcast.104), calls=%async_computation.5 | async-start | bytes 8388608
  104.2 2.5 %slice-start.1 = ((s8[8388608]{0:T(1024)(128)(4,1)}), s8[4194304]{0:T(1024)(128)(4,1)S(1)}, s32[]{:S(2)}) async-start(s8[8388608]{0:T(1024)(128)(4,1)} %bitcast.104), calls=%async_computation.6 | async-start | bytes 8388608
  106.6 44.3 %copy-start.4 = (f32[64,2]{0,1:T(2,128)S(1)}, f32[64,2]{0,1:T(2,128)}, u32[]{:S(2)}) copy-start(f32[64,2]{0,1:T(2,128)} %param.33) | copy-start | bytes 1540
  136.6 14.3 %all-to-all-start.1 = ((bf16[8,2,16,512]{3,2,1,0:T(8,128)(2,1)}), bf16[8,2,16,512]{3,2,1,0:T(8,128)(2,1)S(1)}, u32[]{:S(2)}, u32[]{:S(2)}) async-start(bf16[8,2,16,512]{3,2,1,0:T(8,128)(2,1)} %copy.74), calls=%async_computation.2 | async-start | bytes 524288 | tf_op jit(solution)/shard_map/all_to_all | solution.py:113
Sparse Core Ops, SparseCore 0:
  30.2 35.4 all-gather.2
  109.0 25.8 reduce-scatter.1
